TPU v7x, 32 devices: a whole 2x2x4 slice. The times are simulated.
32 devices in a mesh: ep: 8 (over z, y), tp: 4 (over x, core).
Axes of the slice: x: 2, y: 2, z: 4, core: 2. Of those that a mesh axis runs over, the one named last changes fastest.
Arguments:
- tokens: bfloat16 [2048, 2048], P('ep'), may hold values from -6 to 6
- norm_gain: float32 [2048], replicated, may hold values from 0.1 to 1.9
- expert_ids: int32 [2048, 2], P('ep'), may hold values from 0 to 3, all different within a row; in each aligned block of 256 rows (0 to 255, 256 to 511, ...) at most 160 rows name the same one
- route_weight: float32 [2048, 2], P('ep'), may hold values from 0.2 to 1
- w_gate: bfloat16 [8, 2048, 3584], P('ep', None, 'tp'), may hold values from -0.125 to 0.125
- w_up: bfloat16 [8, 2048, 3584], P('ep', None, 'tp'), may hold values from -0.125 to 0.125
- w_down: bfloat16 [8, 3584, 2048], P('ep', 'tp'), may hold values from -0.0625 to 0.0625
Outputs:
- mixed: bfloat16 [2048, 2048], P('ep', 'tp')
Inputs may be any that keep to these rules, and one draw needn't show every extreme that they name: `expert_ids`: A token names 2 different experts. In each aligned block of 256 tokens (the tokens of one index of ep) no expert is named by more than 160 tokens, a bound that some block reaches.
All inputs are finite; a program needn't handle non-finite values.
Results may differ from a plain program's by a relative error of at most 0.014.
Values may be sent and summed in bfloat16 or wider, within the bound.
A program may use at most 128 MiB of HBM per device.

v0:
```python
import functools

import jax
import jax.numpy as jnp
from jax import lax
from jax.experimental import pallas as pl
from jax.experimental.pallas import tpu as pltpu
from jax.sharding import PartitionSpec as P

HALVES = 2
CORES = 2
EPSILON = 1e-05
MESH = pl.DeviceIdType.MESH


def layer_normed(tokens, norm_gain):
    values = tokens.astype(jnp.float32)
    center = values - jnp.mean(values, axis=-1, keepdims=True)
    spread = jnp.mean(center * center, axis=-1, keepdims=True)
    return (center * lax.rsqrt(spread + EPSILON) * norm_gain).astype(jnp.bfloat16)


def slot_numbers(chosen, experts):
    onehot = (chosen[..., None] == jnp.arange(experts, dtype=jnp.int32)).astype(jnp.int32)
    before = jnp.cumsum(onehot, axis=1) - onehot
    return jnp.sum(before * onehot, axis=-1)


def capacity_of(tok_rows, top_count, experts):
    return 2 * min(tok_rows // 2, 5 * tok_rows * top_count // (8 * experts))


def kernel(experts, cap, tokens_ref, gain_ref, ids_ref, weight_ref, wg_hbm, wu_hbm, wd_hbm,
           out_hbm, wg, wu, wd, out_ref, routed, away, part, mate, chip, hop1, turn, hop2, final, back,
           load_sem, zs, zr, xs, xr, ys, yr, fs, fr, ds, dr, ms, mr, h1s, h1r, h2s, h2r, bs, br):
    ep, tp = lax.axis_index("ep"), lax.axis_index("tp")
    z, y = ep // HALVES, ep % HALVES
    x, c = tp // CORES, tp % CORES
    tok_rows, width = tokens_ref.shape
    quarter = out_ref.shape[1]
    bf16, f32 = jnp.bfloat16, jnp.float32

    loads = [
        pltpu.make_async_copy(src.at[0], dst, load_sem.at[i])
        for i, (src, dst) in enumerate(((wg_hbm, wg), (wu_hbm, wu), (wd_hbm, wd)))
    ]
    for load in loads:
        load.start()

    def device(zz, yy, xx, cc):
        return (zz * HALVES + yy, xx * CORES + cc)

    x_peer = device(z, y, 1 - x, c)
    y_peer = device(z, 1 - y, x, c)
    mate_peer = device(z, y, x, 1 - c)
    first = (z * HALVES + (c * (1 - y) + (1 - c) * y), (c * x + (1 - c) * (1 - x)) * CORES + c)
    second = (z * HALVES + (c * y + (1 - c) * (1 - y)), (c * (1 - x) + (1 - c) * x) * CORES + c)

    def z_peer(o):
        return device((z + o) % experts, y, x, c)

    barrier = pltpu.get_barrier_semaphore()
    peers = [x_peer, y_peer, mate_peer] + [z_peer(o) for o in range(1, experts)]
    for peer in peers:
        pl.semaphore_signal(barrier, inc=1, device_id=peer, device_id_type=MESH)

    ids = jnp.transpose(ids_ref[...])
    one, two = ids[:, 0:1], ids[:, 1:2]
    lane = lax.broadcasted_iota(jnp.int32, (tok_rows, 128), 1)
    expert = (lane + z) % experts
    named = jnp.logical_or(one == expert, two == expert)
    lower = (
        lax.broadcasted_iota(jnp.int32, (tok_rows, tok_rows), 1)
        < lax.broadcasted_iota(jnp.int32, (tok_rows, tok_rows), 0)
    )
    slot = jnp.dot(
        lower.astype(f32).astype(bf16), named.astype(f32).astype(bf16), preferred_element_type=f32
    )
    slot = jnp.where(named, slot, -1.0).astype(jnp.int32)
    places = lax.broadcasted_iota(jnp.int32, (tok_rows, cap), 1)

    def chosen(o):
        return places == slot[:, o:o + 1]

    values = tokens_ref[...].astype(f32)
    mean = jnp.mean(values, axis=-1, keepdims=True)
    center = values - mean
    spread = jnp.mean(center * center, axis=-1, keepdims=True)
    mine = pl.ds(pl.multiple_of(tp * quarter, quarter), quarter)
    own = tokens_ref[:, mine].astype(f32) - mean
    normed = (own * lax.rsqrt(spread + EPSILON) * gain_ref[:, mine]).astype(bf16)

    def outgoing(o):
        return lax.dot_general(
            chosen(o).astype(f32).astype(bf16), normed, (((0,), (0,)), ((), ())),
            preferred_element_type=f32,
        ).astype(bf16)

    def block(d, yy, xx, cc):
        rows = pl.ds(pl.multiple_of(yy * cap, cap), cap)
        columns = pl.ds(pl.multiple_of((xx * CORES + cc) * quarter, quarter), quarter)
        return routed.at[d, rows, columns]

    def send(src, dst, send_sem, recv_sem, peer):
        copy = pltpu.make_async_remote_copy(
            src_ref=src, dst_ref=dst, send_sem=send_sem, recv_sem=recv_sem,
            device_id=peer, device_id_type=MESH,
        )
        copy.start()
        return copy

    order = [0] + sorted(range(1, experts), key=lambda d: -min(d, experts - d))
    turns = order
    for o in order:
        if o:
            away[o - 1] = outgoing(o)
    pl.semaphore_wait(barrier, len(peers))
    z_copies = {}
    for o in order:
        if o:
            d = experts - o
            z_copies[d] = send(away.at[o - 1], block(d, y, x, c), zs.at[d], zr.at[d], z_peer(o))
    routed[0, pl.ds(pl.multiple_of(y * cap, cap), cap), mine] = outgoing(0)

    x_copies, y_copies, forwards, pairs, mates = {}, {}, {}, {}, {}

    def launch(d):
        if d:
            z_copies[d].wait_recv()
        b = block(d, y, x, c)
        x_copies[d] = send(b, b, xs.at[d], xr.at[d], x_peer)
        y_copies[d] = send(b, b, ys.at[d], yr.at[d], y_peer)
        pairs[d] = [send(b, b, ds.at[d, 0], dr.at[d, 0], mate_peer)]

    def relay(d):
        x_copies[d].wait_recv()
        y_copies[d].wait_recv()
        b = block(d, c * y + (1 - c) * (1 - y), c * (1 - x) + (1 - c) * x, c)
        forwards[d] = send(b, b, fs.at[d], fr.at[d], first)
        for i, b in ((1, block(d, y, 1 - x, c)), (2, block(d, 1 - y, x, c))):
            pairs[d].append(send(b, b, ds.at[d, i], dr.at[d, i], mate_peer))

    def finish(d):
        forwards[d].wait_recv()
        b = block(d, 1 - y, 1 - x, c)
        pairs[d].append(send(b, b, ds.at[d, 3], dr.at[d, 3], mate_peer))
        for copy in pairs[d]:
            copy.wait_recv()

    def columns_of(xx, cc):
        return pl.ds(pl.multiple_of((xx * CORES + cc) * quarter, quarter), quarter)

    def compute(d, early, between):
        rows = routed[d]
        gate = jnp.dot(rows, wg[...], preferred_element_type=f32)
        up = jnp.dot(rows, wu[...], preferred_element_type=f32)
        hidden = (gate / (1.0 + jnp.exp(-gate)) * up).astype(bf16)
        between()
        if early:
            loads[2].wait()
        for xx in range(2):
            part[d, 1 - c, xx] = jnp.dot(
                hidden, wd[:, columns_of(xx, 1 - c)], preferred_element_type=f32
            ).astype(bf16)
        mates[d] = send(part.at[d, 1 - c], mate.at[d], ms.at[d], mr.at[d], mate_peer)
        for xx in range(2):
            part[d, c, xx] = jnp.dot(
                hidden, wd[:, columns_of(xx, c)], preferred_element_type=f32
            ).astype(bf16)

    hop1_copies, hop2_copies, back_copies = {}, {}, {}

    def return_first(d):
        mates[d].wait_recv()
        for j in (2, 3, 0, 1):
            low, high = j % 2, j // 2
            x_low, x_high = (1 - x if low else x), (1 - x if high else x)
            y_low, y_high = (1 - y if low else y), (1 - y if high else y)
            xx = c * x_low + (1 - c) * x_high
            yy = c * y_high + (1 - c) * y_low
            rows = pl.ds(pl.multiple_of(yy * cap, cap), cap)
            chip[d, j] = (part[d, c, xx, rows].astype(f32) + mate[d, xx, rows].astype(f32)).astype(bf16)
            if j == 3:
                hop1_copies[d] = send(chip.at[d, pl.ds(2, 2)], hop1.at[d], h1s.at[d], h1r.at[d], first)

    def return_second(d):
        hop1_copies[d].wait_recv()
        turn[d] = (chip[d, 1].astype(f32) + hop1[d, 1].astype(f32)).astype(bf16)
        hop2_copies[d] = send(turn.at[d], hop2.at[d], h2s.at[d], h2r.at[d], second)

    def return_third(d):
        hop2_copies[d].wait_recv()
        total = chip[d, 0].astype(f32) + hop1[d, 0].astype(f32) + hop2[d].astype(f32)
        if d == 0:
            back[0] = total.astype(bf16)
        else:
            final[d] = total.astype(bf16)
            o = experts - d
            back_copies[d] = send(final.at[d], back.at[o], bs.at[o], br.at[o], z_peer(d))

    look = 2
    for k in range(look):
        launch(order[k])
    for k in range(look - 1):
        relay(order[k])

    def ahead(k):
        if k + look < experts:
            launch(order[k + look])
        if k + look - 1 < experts:
            relay(order[k + look - 1])

    for k, d in enumerate(turns):
        def between(k=k):
            pass
            if k >= 1:
                return_second(turns[k - 1])

        ahead(k)
        finish(d)
        if k == 0:
            loads[0].wait()
            loads[1].wait()
        compute(d, k == 0, between)
        return_first(d)
        if k >= 2:
            return_third(turns[k - 2])
    return_second(turns[-1])
    return_third(turns[-2])
    return_third(turns[-1])

    total = jnp.zeros((tok_rows, quarter), f32)
    route = jnp.transpose(weight_ref[...])
    for o in order:
        if o:
            back_copies[experts - o].wait_recv()
        e = (z + o) % experts
        share = jnp.where(one == e, route[:, 0:1], 0.0) + jnp.where(two == e, route[:, 1:2], 0.0)
        mix = jnp.where(chosen(o), share, 0.0)
        high = mix.astype(bf16)
        low = (mix - high.astype(f32)).astype(bf16)
        rows = back[o]
        total += jnp.dot(high, rows, preferred_element_type=f32)
        total += jnp.dot(low, rows, preferred_element_type=f32)
    out_ref[...] = total.astype(bf16)
    store = pltpu.make_async_copy(out_ref, out_hbm, load_sem.at[3])
    store.start()

    for group in (z_copies, x_copies, y_copies, forwards, mates, hop1_copies, hop2_copies, back_copies):
        for d in group:
            group[d].wait_send()
    for d in pairs:
        for copy in pairs[d]:
            copy.wait_send()
    store.wait()


def fused_body(tokens, norm_gain, expert_ids, route_weight, w_gate, w_up, w_down):
    tok_rows, width = tokens.shape
    experts = lax.axis_size("ep") // HALVES
    cap = capacity_of(tok_rows, expert_ids.shape[1], experts)
    tp_count = lax.axis_size("tp")
    quarter = width // tp_count
    units = w_gate.shape[2]
    bf16 = jnp.bfloat16
    dma = pltpu.SemaphoreType.DMA
    vmem = pl.BlockSpec(memory_space=pltpu.VMEM)
    hbm = pl.BlockSpec(memory_space=pl.ANY)
    one = dma((experts,))
    return pl.pallas_call(
        functools.partial(kernel, experts, cap),
        out_shape=jax.ShapeDtypeStruct((tok_rows, quarter), bf16),
        in_specs=[vmem, vmem, vmem, vmem, hbm, hbm, hbm],
        out_specs=hbm,
        scratch_shapes=[
            pltpu.VMEM((width, units), bf16),
            pltpu.VMEM((width, units), bf16),
            pltpu.VMEM((units, width), bf16),
            pltpu.VMEM((tok_rows, quarter), bf16),
            pltpu.VMEM((experts, HALVES * cap, width), bf16),
            pltpu.VMEM((experts - 1, cap, quarter), bf16),
            pltpu.VMEM((experts, CORES, 2, HALVES * cap, quarter), bf16),
            pltpu.VMEM((experts, 2, HALVES * cap, quarter), bf16),
            pltpu.VMEM((experts, 4, cap, quarter), bf16),
            pltpu.VMEM((experts, 2, cap, quarter), bf16),
            pltpu.VMEM((experts, cap, quarter), bf16),
            pltpu.VMEM((experts, cap, quarter), bf16),
            pltpu.VMEM((experts, cap, quarter), bf16),
            pltpu.VMEM((experts, cap, quarter), bf16),
            dma((4,)),
            one, one, one, one, one, one, one, one,
            dma((experts, 4)), dma((experts, 4)),
            one, one, one, one, one, one, one, one,
        ],
        compiler_params=pltpu.CompilerParams(
            collective_id=0, has_side_effects=True, vmem_limit_bytes=60 * 1024 * 1024
        ),
        name="expert_layer",
    )(tokens, norm_gain.reshape(1, -1), expert_ids.T, route_weight.T, w_gate, w_up, w_down)


def body(tokens, norm_gain, expert_ids, route_weight, w_gate, w_up, w_down):
    tok_rows, width = tokens.shape
    top_count = expert_ids.shape[1]
    ep_count = lax.axis_size("ep")
    experts = ep_count // HALVES
    capacity = capacity_of(tok_rows, top_count, experts)
    normed = layer_normed(tokens, norm_gain)
    padded = jnp.concatenate([normed, jnp.zeros((1, width), jnp.bfloat16)], axis=0)
    slots = slot_numbers(expert_ids.reshape(1, -1), experts).reshape(-1)
    flat_expert = expert_ids.reshape(-1)
    owner = jnp.arange(tok_rows * top_count, dtype=jnp.int32) // top_count
    place = flat_expert * capacity + slots
    table = jnp.full((experts * capacity,), tok_rows, jnp.int32).at[place].set(owner)
    outgoing = padded[table].reshape(experts, capacity, width)
    columns = width // lax.axis_size("tp")
    portion = lax.dynamic_slice_in_dim(outgoing, lax.axis_index("tp") * columns, columns, 2)
    doubled = jnp.repeat(portion, HALVES, axis=0)
    pieces = lax.all_to_all(doubled, "ep", split_axis=0, concat_axis=0, tiled=True)
    arrived = lax.all_gather(pieces, "tp", axis=2, tiled=True)
    routed = arrived.reshape(-1, width)
    gate = jnp.dot(routed, w_gate[0], preferred_element_type=jnp.float32)
    up = jnp.dot(routed, w_up[0], preferred_element_type=jnp.float32)
    hidden = (jax.nn.silu(gate) * up).astype(jnp.bfloat16)
    partial_value = jnp.dot(hidden, w_down[0], preferred_element_type=jnp.float32)
    reduced = lax.psum_scatter(
        partial_value.astype(jnp.bfloat16), "tp", scatter_dimension=1, tiled=True
    )
    returned = lax.all_to_all(
        reduced.reshape(ep_count, capacity, -1), "ep", split_axis=0, concat_axis=0, tiled=True
    )
    quarter = returned.shape[2]
    summed = returned.reshape(experts, HALVES, capacity, quarter).astype(jnp.float32).sum(axis=1)
    picked = summed.reshape(experts * capacity, quarter)[place].reshape(
        tok_rows, top_count, quarter
    )
    mixed = jnp.sum(route_weight[:, :, None] * picked, axis=1)
    return mixed.astype(jnp.bfloat16)


def choose(*args):
    tok_rows = args[0].shape[0]
    experts = lax.axis_size("ep") // HALVES
    cap = capacity_of(tok_rows, args[2].shape[1], experts)
    if cap % 16 == 0 and lax.axis_size("tp") == 2 * CORES and args[2].shape[1] == 2:
        return fused_body(*args)
    return body(*args)


def solution(mesh):
    return jax.shard_map(
        choose,
        mesh=mesh,
        in_specs=(
            P("ep", None),
            P(),
            P("ep", None),
            P("ep", None),
            P("ep", None, "tp"),
            P("ep", None, "tp"),
            P("ep", "tp", None),
        ),
        out_specs=P("ep", "tp"),
        check_vma=False,
    )
```

profile of v0, /device:TPU:0, one launch (start us, length us, event | category | flops | bytes accessed | tf_op | source)
XLA Modules:
  0.0 79.6 jit_solution(5490597525705432121)
XLA Ops:
  0.0 77.9 %expert_layer.1 = bf16[256,512]{1,0:T(8,128)(2,1)} custom-call(bf16[256,2048]{1,0:T(8,128)(2,1)} %tokens_ref.1, f32[1,2048]{1,0:T(1,128)} %bitcast.3, s32[2,256]{1,0:T(2,128)} %bitcast.4, f32[2,256]{1,0:T(2,128)} %bitcast.5, bf16[1,2048,896]{2,1,0:T(8,128)(2,1)} %wg_hbm.1, bf16[1,2048,896]{2,1,0:T(8,128)(2,1)} %wu_hbm.1, bf16[1,896,2048]{2,1,0:T(8,128)(2,1)} %wd_hbm.1), custom_call_target="tpu_custom_call" | custom-call | tf_op jit(solution)/shard_map/expert_layer/pallas_call | solution.py:270
  77.9 1.7 %copy.9 = bf16[256,512]{1,0:T(8,128)(2,1)} copy(bf16[256,512]{1,0:T(8,128)(2,1)} %expert_layer.1) | data formatting | bytes 524288
where the time goes:
time: 79.8 us; the launch traced here: 79.6 us
  Pallas kernels  77.9 us (98%)
  local copies, waits for them, and re-layouts  1.67 us (2%)
    pallas_call x1, Pallas kernels, fused_body(): pl.pallas_call(functools.partial(kernel, experts, cap), out_shape=jax.Sha...  77.9 us
    unnamed x1, local copies, waits for them, and re-layouts  1.67 us

commit v1 on v0

v1 whole, which is shorter than its diff:
```python
import functools

import jax
import jax.numpy as jnp
from jax import lax
from jax.experimental import pallas as pl
from jax.experimental.pallas import tpu as pltpu
from jax.sharding import PartitionSpec as P

HALVES = 2
CORES = 2
EPSILON = 1e-05
MESH = pl.DeviceIdType.MESH
ORDER = (
    ('own_rest',),
    ('join', 0),
    ('expand', 0, 0),
    ('join', 1),
    ('launch', 1),
    ('launch', 2),
    ('expand', 0, 1),
    ('relay', 1),
    ('launch', 3),
    ('share', 1),
    ('shrink', 0, (1,)),
    ('finish', 1),
    ('relay', 2),
    ('expand', 1, 0),
    ('relay', 3),
    ('expand', 1, 1),
    ('shrink', 0, (0,)),
    ('shrink', 0, (2,)),
    ('shrink', 1, (0,)),
    ('share', 3),
    ('shrink', 1, (3,)),
    ('shrink', 1, (2,)),
    ('finish', 3),
    ('share', 2),
    ('expand', 3, 0),
    ('expand', 3, 1),
    ('shrink', 1, (1,)),
    ('second', 1),
    ('expand', 2, 0),
    ('shrink', 3, (3,)),
    ('finish', 2),
    ('shrink', 3, (1,)),
    ('shrink', 3, (2,)),
    ('third', 1),
    ('expand', 2, 1),
    ('second', 3),
    ('shrink', 3, (0,)),
    ('shrink', 2, (2,)),
    ('shrink', 2, (3,)),
    ('shrink', 2, (1,)),
    ('third', 3),
    ('shrink', 0, (3,)),
    ('shrink', 2, (0,)),
    ('second', 2),
    ('mix', 1),
    ('second', 0),
    ('third', 2),
    ('mix', 3),
    ('third', 0),
    ('mix', 0),
    ('mix', 2),
)
PARTNERS = ((2, 1, 3), (3, 0, 2))
MIXES = (1, 3, 0, 2)


def layer_normed(tokens, norm_gain):
    values = tokens.astype(jnp.float32)
    center = values - jnp.mean(values, axis=-1, keepdims=True)
    spread = jnp.mean(center * center, axis=-1, keepdims=True)
    return (center * lax.rsqrt(spread + EPSILON) * norm_gain).astype(jnp.bfloat16)


def slot_numbers(chosen, experts):
    onehot = (chosen[..., None] == jnp.arange(experts, dtype=jnp.int32)).astype(jnp.int32)
    before = jnp.cumsum(onehot, axis=1) - onehot
    return jnp.sum(before * onehot, axis=-1)


def capacity_of(tok_rows, top_count, experts):
    return 2 * min(tok_rows // 2, 5 * tok_rows * top_count // (8 * experts))


def kernel(experts, cap, tokens_ref, gain_ref, ids_ref, weight_ref, wg_hbm, wu_hbm, wd_hbm,
           out_hbm, wgu, wdc, out_ref, normed, picks, routed, away, hid, chip, hop1, turn, hop2, final, back, total,
           load_sem, ws, wr, zs, zr, as_, ar, ams, amr, xs, xr, fs, fr, ds, dr, hs, hr,
           h1s, h1r, h2s, h2r, bs, br):
    ep, tp = lax.axis_index("ep"), lax.axis_index("tp")
    z, y = ep // HALVES, ep % HALVES
    x, c = tp // CORES, tp % CORES
    tok_rows, width = tokens_ref.shape
    quarter = out_ref.shape[1]
    units = wdc.shape[0] // CORES
    bf16, f32 = jnp.bfloat16, jnp.float32

    def columns_of(xx, cc):
        return pl.ds(pl.multiple_of((xx * CORES + cc) * quarter, quarter), quarter)

    def rows_of(yy):
        return pl.ds(pl.multiple_of(yy * cap, cap), cap)

    own_units, mate_units = pl.ds(0, units), pl.ds(units, units)
    loads = [
        pltpu.make_async_copy(wg_hbm.at[0], wgu.at[:, own_units], load_sem.at[0]),
        pltpu.make_async_copy(wu_hbm.at[0], wgu.at[:, mate_units], load_sem.at[1]),
    ] + [
        pltpu.make_async_copy(
            wd_hbm.at[0, :, columns_of(xx, c)], wdc.at[own_units, pl.ds(xx * quarter, quarter)], load_sem.at[2 + xx]
        )
        for xx in range(2)
    ]
    for load in loads:
        load.start()

    def device(zz, yy, xx, cc):
        return (zz * HALVES + yy, xx * CORES + cc)

    x_peer = device(z, y, 1 - x, c)
    y_peer = device(z, 1 - y, x, c)
    mate_peer = device(z, y, x, 1 - c)
    first = (z * HALVES + (c * (1 - y) + (1 - c) * y), (c * x + (1 - c) * (1 - x)) * CORES + c)
    second = (z * HALVES + (c * y + (1 - c) * (1 - y)), (c * (1 - x) + (1 - c) * x) * CORES + c)

    plane = [z] + [nearest(z, k, experts) for k in range(experts - 1)]

    barrier = pltpu.get_barrier_semaphore()
    peers = [x_peer, y_peer, mate_peer] + [device(p, y, x, c) for p in plane[1:]]
    for peer in peers:
        pl.semaphore_signal(barrier, inc=1, device_id=peer, device_id_type=MESH)

    ids = jnp.transpose(ids_ref[...])
    one, two = ids[:, 0:1], ids[:, 1:2]
    lane = lax.broadcasted_iota(jnp.int32, (tok_rows, 128), 1)
    places = lax.broadcasted_iota(jnp.int32, (tok_rows, cap), 1)
    expert = jnp.full((tok_rows, 128), -1, jnp.int32)
    for k, p in enumerate(plane):
        expert = jnp.where(lane == k, p, expert)
    named = jnp.logical_or(one == expert, two == expert)
    lower = (
        lax.broadcasted_iota(jnp.int32, (tok_rows, tok_rows), 1)
        < lax.broadcasted_iota(jnp.int32, (tok_rows, tok_rows), 0)
    )
    slot = jnp.dot(
        lower.astype(f32).astype(bf16), named.astype(f32).astype(bf16), preferred_element_type=f32
    )
    slot = jnp.where(named, slot, -1.0).astype(jnp.int32)

    values = tokens_ref[...].astype(f32)
    mean = jnp.mean(values, axis=-1, keepdims=True)
    center = values - mean
    spread = jnp.mean(center * center, axis=-1, keepdims=True)
    scale = lax.rsqrt(spread + EPSILON)

    def norm(columns):
        own = tokens_ref[:, columns].astype(f32) - mean
        normed[:, columns] = (own * scale * gain_ref[:, columns]).astype(bf16)

    def pick(k, columns):
        return lax.dot_general(
            picks[k], normed[:, columns], (((0,), (0,)), ((), ())), preferred_element_type=f32
        ).astype(bf16)

    mine = columns_of(x, c)
    norm(mine)
    for k in range(1, experts):
        picks[k] = (places == slot[:, k:k + 1]).astype(f32).astype(bf16)
        away[k - 1] = pick(k, mine)
    picks[0] = (places == slot[:, 0:1]).astype(f32).astype(bf16)
    here = routed.at[z, rows_of(y)]
    here[:, mine] = pick(0, mine)
    norm(columns_of(1 - x, c))
    here[:, columns_of(1 - x, c)] = pick(0, columns_of(1 - x, c))

    sent = []

    def send(src, dst, send_sem, recv_sem, peer):
        copy = pltpu.make_async_remote_copy(
            src_ref=src, dst_ref=dst, send_sem=send_sem, recv_sem=recv_sem,
            device_id=peer, device_id_type=MESH,
        )
        copy.start()
        sent.append(copy)
        return copy

    def block(p, yy, xx, cc):
        return routed.at[plane[p], rows_of(yy), columns_of(xx, cc)]

    pl.semaphore_wait(barrier, len(peers))
    for k in range(1, experts):
        send(away.at[k - 1], routed.at[z, rows_of(y), mine], zs.at[k - 1], zr.at[z], device(plane[k], y, x, c))
    for i, xx in enumerate((x, 1 - x)):
        b = block(0, y, xx, c)
        send(b, b, as_.at[i], ar.at[i], y_peer)
    w_copies = [
        send(wd_hbm.at[0, :, columns_of(xx, 1 - c)], wdc.at[mate_units, pl.ds(xx * quarter, quarter)],
             ws.at[xx], wr.at[xx], mate_peer)
        for xx in range(2)
    ]

    def arrived(dst, sem):
        pltpu.make_async_remote_copy(
            src_ref=dst, dst_ref=dst, send_sem=zs.at[0], recv_sem=sem,
            device_id=mate_peer, device_id_type=MESH,
        ).wait_recv()

    handed, ready = {}, set()
    hop1_copies, hop2_copies = {}, {}

    def own_rest():
        for xx in (x, 1 - x):
            columns = columns_of(xx, 1 - c)
            norm(columns)
            here[:, columns] = pick(0, columns)

    def join(i):
        xx = 1 - x if i else x
        b = block(0, 1 - y, xx, c)
        arrived(b, ar.at[i])
        send(b, b, ams.at[i], amr.at[i], mate_peer)

    def launch(p):
        b = block(p, y, x, c)
        arrived(b, zr.at[plane[p]])
        send(b, b, xs.at[p, 0], xr.at[p, 0], x_peer)
        send(b, b, xs.at[p, 1], xr.at[p, 1], y_peer)
        send(b, b, ds.at[p, 0], dr.at[p, 0], mate_peer)

    def relay(p):
        b = block(p, c * y + (1 - c) * (1 - y), c * (1 - x) + (1 - c) * x, c)
        arrived(b, xr.at[p, 1 - c])
        send(b, b, fs.at[p], fr.at[p], first)
        send(b, b, ds.at[p, 2 - c], dr.at[p, 2 - c], mate_peer)

    def share(p):
        b = block(p, (1 - c) * y + c * (1 - y), (1 - c) * (1 - x) + c * x, c)
        arrived(b, xr.at[p, c])
        send(b, b, ds.at[p, 1 + c], dr.at[p, 1 + c], mate_peer)

    def finish(p):
        b = block(p, 1 - y, 1 - x, c)
        arrived(b, fr.at[p])
        send(b, b, ds.at[p, 3], dr.at[p, 3], mate_peer)

    def expand(p, i):
        if p == 0 and i == 0:
            loads[0].wait()
            loads[1].wait()
        rows = rows_of(1 - y if i else y)
        if p == 0 and i == 1:
            arrived(block(0, 1 - y, x, 1 - c), amr.at[0])
            arrived(block(0, 1 - y, 1 - x, 1 - c), amr.at[1])
        elif p and i == 0:
            arrived(block(p, y, x, 1 - c), dr.at[p, 0])
            arrived(block(p, y, 1 - x, 1 - c), dr.at[p, 1])
        elif p:
            arrived(block(p, 1 - y, x, 1 - c), dr.at[p, 2])
            arrived(block(p, 1 - y, 1 - x, 1 - c), dr.at[p, 3])
        both = jnp.dot(routed[plane[p], rows], wgu[...], preferred_element_type=f32)
        gate, up = both[:, :units], both[:, units:]
        hid[p, rows, own_units] = (gate / (1.0 + jnp.exp(-gate)) * up).astype(bf16)
        handed[p, i] = send(
            hid.at[p, rows, own_units], hid.at[p, rows, mate_units], hs.at[p, i], hr.at[p, i], mate_peer
        )

    def shrink(p, js):
        if not ready:
            for copy in loads[2:]:
                copy.wait()
            for copy in w_copies:
                copy.wait_recv()
        if p not in ready:
            ready.add(p)
            for i in range(2):
                handed[p, i].wait_recv()
        for j in js:
            low, high = j % 2, j // 2
            x_low, x_high = (1 - x if low else x), (1 - x if high else x)
            y_low, y_high = (1 - y if low else y), (1 - y if high else y)
            xx = c * x_low + (1 - c) * x_high
            yy = c * y_high + (1 - c) * y_low
            chip[p, j] = jnp.dot(
                hid[p, rows_of(yy)], wdc[:, pl.ds(pl.multiple_of(xx * quarter, quarter), quarter)],
                preferred_element_type=f32,
            ).astype(bf16)
            if j >= 2:
                hop1_copies[p, j - 2] = send(
                    chip.at[p, j], hop1.at[p, j - 2], h1s.at[p, j - 2], h1r.at[p, j - 2], first
                )

    def return_second(p):
        hop1_copies[p, 1].wait_recv()
        turn[p] = (chip[p, 1].astype(f32) + hop1[p, 1].astype(f32)).astype(bf16)
        hop2_copies[p] = send(turn.at[p], hop2.at[p], h2s.at[p], h2r.at[p], second)

    def return_third(p):
        hop1_copies[p, 0].wait_recv()
        part = chip[p, 0].astype(f32) + hop1[p, 0].astype(f32)
        hop2_copies[p].wait_recv()
        part = (part + hop2[p].astype(f32)).astype(bf16)
        if p == 0:
            back[z] = part
        else:
            final[p - 1] = part
            send(final.at[p - 1], back.at[z], bs.at[p - 1], br.at[z], device(plane[p], y, x, c))

    def mix(p):
        e = plane[p]
        if p:
            arrived(back.at[e], br.at[e])
        route = jnp.transpose(weight_ref[...])
        share = jnp.where(one == e, route[:, 0:1], 0.0) + jnp.where(two == e, route[:, 1:2], 0.0)
        value = share * jnp.dot(picks[p], back[e], preferred_element_type=f32)
        if p == MIXES[0]:
            total[...] = value
        elif p != MIXES[-1]:
            total[...] += value
        else:
            out_ref[...] = (total[...] + value).astype(bf16)

    steps = dict(own_rest=own_rest, join=join, launch=launch, relay=relay, share=share, finish=finish, expand=expand,
                 shrink=shrink, second=return_second, third=return_third, mix=mix)
    for name, *arguments in ORDER:
        steps[name](*arguments)

    store = pltpu.make_async_copy(out_ref, out_hbm, load_sem.at[4])
    store.start()
    for copy in sent:
        copy.wait_send()
    store.wait()


def nearest(z, k, experts):
    place = 0
    for zz in range(experts):
        near = zz if zz < experts - 1 - zz else experts - 1 - zz
        other = PARTNERS[near][k]
        place = place + jnp.where(z == zz, other if near == zz else experts - 1 - other, 0)
    return place


def fused_body(tokens, norm_gain, expert_ids, route_weight, w_gate, w_up, w_down):
    tok_rows, width = tokens.shape
    experts = lax.axis_size("ep") // HALVES
    cap = capacity_of(tok_rows, expert_ids.shape[1], experts)
    tp_count = lax.axis_size("tp")
    quarter = width // tp_count
    units = w_gate.shape[2]
    bf16 = jnp.bfloat16
    dma = pltpu.SemaphoreType.DMA
    vmem = pl.BlockSpec(memory_space=pltpu.VMEM)
    hbm = pl.BlockSpec(memory_space=pl.ANY)
    one, two = dma((experts,)), dma((experts, 2))
    return pl.pallas_call(
        functools.partial(kernel, experts, cap),
        out_shape=jax.ShapeDtypeStruct((tok_rows, quarter), bf16),
        in_specs=[vmem, vmem, vmem, vmem, hbm, hbm, hbm],
        out_specs=hbm,
        scratch_shapes=[
            pltpu.VMEM((width, 2 * units), bf16),
            pltpu.VMEM((CORES * units, 2 * quarter), bf16),
            pltpu.VMEM((tok_rows, quarter), bf16),
            pltpu.VMEM((tok_rows, width), bf16),
            pltpu.VMEM((experts, tok_rows, cap), bf16),
            pltpu.VMEM((experts, HALVES * cap, width), bf16),
            pltpu.VMEM((experts - 1, cap, quarter), bf16),
            pltpu.VMEM((experts, HALVES * cap, CORES * units), bf16),
            pltpu.VMEM((experts, 4, cap, quarter), bf16),
            pltpu.VMEM((experts, 2, cap, quarter), bf16),
            pltpu.VMEM((experts, cap, quarter), bf16),
            pltpu.VMEM((experts, cap, quarter), bf16),
            pltpu.VMEM((experts - 1, cap, quarter), bf16),
            pltpu.VMEM((experts, cap, quarter), bf16),
            pltpu.VMEM((tok_rows, quarter), jnp.float32),
            dma((5,)),
            dma((2,)), dma((2,)),
            one, one,
            dma((2,)), dma((2,)), dma((2,)), dma((2,)),
            two, two, one, one,
            dma((experts, 4)), dma((experts, 4)),
            two, two,
            two, two, one, one, one, one,
        ],
        compiler_params=pltpu.CompilerParams(
            collective_id=0, has_side_effects=True, vmem_limit_bytes=60 * 1024 * 1024
        ),
        name="expert_layer",
    )(tokens, norm_gain.reshape(1, -1), expert_ids.T, route_weight.T, w_gate, w_up, w_down)


def body(tokens, norm_gain, expert_ids, route_weight, w_gate, w_up, w_down):
    tok_rows, width = tokens.shape
    top_count = expert_ids.shape[1]
    ep_count = lax.axis_size("ep")
    experts = ep_count // HALVES
    capacity = capacity_of(tok_rows, top_count, experts)
    normed = layer_normed(tokens, norm_gain)
    padded = jnp.concatenate([normed, jnp.zeros((1, width), jnp.bfloat16)], axis=0)
    slots = slot_numbers(expert_ids.reshape(1, -1), experts).reshape(-1)
    flat_expert = expert_ids.reshape(-1)
    owner = jnp.arange(tok_rows * top_count, dtype=jnp.int32) // top_count
    place = flat_expert * capacity + slots
    table = jnp.full((experts * capacity,), tok_rows, jnp.int32).at[place].set(owner)
    outgoing = padded[table].reshape(experts, capacity, width)
    columns = width // lax.axis_size("tp")
    portion = lax.dynamic_slice_in_dim(outgoing, lax.axis_index("tp") * columns, columns, 2)
    doubled = jnp.repeat(portion, HALVES, axis=0)
    pieces = lax.all_to_all(doubled, "ep", split_axis=0, concat_axis=0, tiled=True)
    arrived = lax.all_gather(pieces, "tp", axis=2, tiled=True)
    routed = arrived.reshape(-1, width)
    gate = jnp.dot(routed, w_gate[0], preferred_element_type=jnp.float32)
    up = jnp.dot(routed, w_up[0], preferred_element_type=jnp.float32)
    hidden = (jax.nn.silu(gate) * up).astype(jnp.bfloat16)
    partial_value = jnp.dot(hidden, w_down[0], preferred_element_type=jnp.float32)
    reduced = lax.psum_scatter(
        partial_value.astype(jnp.bfloat16), "tp", scatter_dimension=1, tiled=True
    )
    returned = lax.all_to_all(
        reduced.reshape(ep_count, capacity, -1), "ep", split_axis=0, concat_axis=0, tiled=True
    )
    quarter = returned.shape[2]
    summed = returned.reshape(experts, HALVES, capacity, quarter).astype(jnp.float32).sum(axis=1)
    picked = summed.reshape(experts * capacity, quarter)[place].reshape(
        tok_rows, top_count, quarter
    )
    mixed = jnp.sum(route_weight[:, :, None] * picked, axis=1)
    return mixed.astype(jnp.bfloat16)


def choose(*args):
    tok_rows = args[0].shape[0]
    experts = lax.axis_size("ep") // HALVES
    cap = capacity_of(tok_rows, args[2].shape[1], experts)
    if experts == len(MIXES) and cap % 16 == 0 and lax.axis_size("tp") == 2 * CORES and args[2].shape[1] == 2:
        return fused_body(*args)
    return body(*args)


def solution(mesh):
    return jax.shard_map(
        choose,
        mesh=mesh,
        in_specs=(
            P("ep", None),
            P(),
            P("ep", None),
            P("ep", None),
            P("ep", None, "tp"),
            P("ep", None, "tp"),
            P("ep", "tp", None),
        ),
        out_specs=P("ep", "tp"),
        check_vma=False,
    )
```

time: 79.8 us -> 67 us (0.84)
  Pallas kernels: 77.9 us -> 65.2 us
    pallas_call x1, Pallas kernels: 77.9 us -> 65.2 us  [fused_body(): pl.pallas_call(functools.partial(kernel, experts, cap), out_shape=jax.Sha...]
where the time goes in v1:
time: 67 us; the launch traced here: 66.8 us
  Pallas kernels  65.2 us (97%)
  local copies, waits for them, and re-layouts  1.67 us (2%)
    pallas_call x1, Pallas kernels, fused_body(): pl.pallas_call(functools.partial(kernel, experts, cap), out_shape=jax.Sha...  65.2 us
    unnamed x1, local copies, waits for them, and re-layouts  1.67 us

profile of v1, /device:TPU:0, one launch (start us, length us, event | category | flops | bytes accessed | tf_op | source)
XLA Modules:
  0.0 66.8 jit_solution(5029225614301910368)
XLA Ops:
  0.0 65.2 %expert_layer.1 = bf16[256,512]{1,0:T(8,128)(2,1)} custom-call(bf16[256,2048]{1,0:T(8,128)(2,1)} %tokens_ref.1, f32[1,2048]{1,0:T(1,128)} %bitcast.3, s32[2,256]{1,0:T(2,128)} %bitcast.4, f32[2,256]{1,0:T(2,128)} %bitcast.5, bf16[1,2048,896]{2,1,0:T(8,128)(2,1)} %wg_hbm.1, bf16[1,2048,896]{2,1,0:T(8,128)(2,1)} %wu_hbm.1, bf16[1,896,2048]{2,1,0:T(8,128)(2,1)} %wd_hbm.1), custom_call_target="tpu_custom_call" | custom-call | tf_op jit(solution)/shard_map/expert_layer/pallas_call | solution.py:357
  65.2 1.7 %copy.9 = bf16[256,512]{1,0:T(8,128)(2,1)} copy(bf16[256,512]{1,0:T(8,128)(2,1)} %expert_layer.1) | data formatting | bytes 524288

commit v2 on v1

--- a/solution.py
+++ b/solution.py
@@ -12,60 +12,62 @@
 EPSILON = 1e-05
 MESH = pl.DeviceIdType.MESH
 ORDER = (
+    ('join', 0),
     ('own_rest',),
-    ('join', 0),
+    ('launch', 1),
+    ('join', 1),
+    ('wsend',),
     ('expand', 0, 0),
-    ('join', 1),
-    ('launch', 1),
     ('launch', 2),
     ('expand', 0, 1),
     ('relay', 1),
+    ('share', 1),
+    ('expand', 1, 0),
     ('launch', 3),
-    ('share', 1),
-    ('shrink', 0, (1,)),
     ('finish', 1),
+    ('shrink', 0, (0,)),
     ('relay', 2),
-    ('expand', 1, 0),
+    ('share', 2),
+    ('expand', 1, 1),
+    ('share', 3),
     ('relay', 3),
-    ('expand', 1, 1),
-    ('shrink', 0, (0,)),
-    ('shrink', 0, (2,)),
-    ('shrink', 1, (0,)),
-    ('share', 3),
     ('shrink', 1, (3,)),
     ('shrink', 1, (2,)),
+    ('expand', 3, 0),
+    ('shrink', 1, (1,)),
+    ('finish', 2),
     ('finish', 3),
-    ('share', 2),
-    ('expand', 3, 0),
+    ('expand', 2, 0),
+    ('second', 1),
     ('expand', 3, 1),
-    ('shrink', 1, (1,)),
-    ('second', 1),
-    ('expand', 2, 0),
+    ('shrink', 0, (3,)),
+    ('shrink', 1, (0,)),
     ('shrink', 3, (3,)),
-    ('finish', 2),
+    ('third', 1),
+    ('shrink', 3, (2,)),
     ('shrink', 3, (1,)),
-    ('shrink', 3, (2,)),
-    ('third', 1),
+    ('shrink', 0, (1,)),
     ('expand', 2, 1),
     ('second', 3),
     ('shrink', 3, (0,)),
+    ('shrink', 2, (1,)),
+    ('shrink', 2, (3,)),
     ('shrink', 2, (2,)),
-    ('shrink', 2, (3,)),
-    ('shrink', 2, (1,)),
     ('third', 3),
-    ('shrink', 0, (3,)),
+    ('second', 2),
+    ('second', 0),
     ('shrink', 2, (0,)),
-    ('second', 2),
     ('mix', 1),
-    ('second', 0),
+    ('shrink', 0, (2,)),
     ('third', 2),
-    ('mix', 3),
     ('third', 0),
     ('mix', 0),
+    ('mix', 3),
     ('mix', 2),
 )
 PARTNERS = ((2, 1, 3), (3, 0, 2))
-MIXES = (1, 3, 0, 2)
+PICKS = (1, 0, 2, 3)
+MIXES = (1, 0, 3, 2)
 
 
 def layer_normed(tokens, norm_gain):
@@ -166,14 +168,6 @@
 
     mine = columns_of(x, c)
     norm(mine)
-    for k in range(1, experts):
-        picks[k] = (places == slot[:, k:k + 1]).astype(f32).astype(bf16)
-        away[k - 1] = pick(k, mine)
-    picks[0] = (places == slot[:, 0:1]).astype(f32).astype(bf16)
-    here = routed.at[z, rows_of(y)]
-    here[:, mine] = pick(0, mine)
-    norm(columns_of(1 - x, c))
-    here[:, columns_of(1 - x, c)] = pick(0, columns_of(1 - x, c))
 
     sent = []
 
@@ -189,17 +183,33 @@
     def block(p, yy, xx, cc):
         return routed.at[plane[p], rows_of(yy), columns_of(xx, cc)]
 
+    half = cap // 2
+
+    def piece(yy, xx, i):
+        return routed.at[z, pl.ds(pl.multiple_of(yy * cap + i * half, half), half), columns_of(xx, c)]
+
+    here = routed.at[z, rows_of(y)]
     pl.semaphore_wait(barrier, len(peers))
-    for k in range(1, experts):
-        send(away.at[k - 1], routed.at[z, rows_of(y), mine], zs.at[k - 1], zr.at[z], device(plane[k], y, x, c))
-    for i, xx in enumerate((x, 1 - x)):
-        b = block(0, y, xx, c)
-        send(b, b, as_.at[i], ar.at[i], y_peer)
-    w_copies = [
-        send(wd_hbm.at[0, :, columns_of(xx, 1 - c)], wdc.at[mate_units, pl.ds(xx * quarter, quarter)],
-             ws.at[xx], wr.at[xx], mate_peer)
-        for xx in range(2)
-    ]
+    for k in PICKS:
+        picks[k] = (places == slot[:, k:k + 1]).astype(f32).astype(bf16)
+        if k:
+            away[k - 1] = pick(k, mine)
+            send(away.at[k - 1], routed.at[z, rows_of(y), mine], zs.at[k - 1], zr.at[z],
+                 device(plane[k], y, x, c))
+        else:
+            here[:, mine] = pick(0, mine)
+            for i in range(2):
+                send(piece(y, x, i), piece(y, x, i), as_.at[i], ar.at[i], y_peer)
+    norm(columns_of(1 - x, c))
+    here[:, columns_of(1 - x, c)] = pick(0, columns_of(1 - x, c))
+    b = piece(y, 1 - x, 1)
+    send(b, b, as_.at[2], ar.at[2], y_peer)
+
+    def hand_down():
+        for xx in range(2):
+            w_copies.append(send(
+                wd_hbm.at[0, :, columns_of(xx, 1 - c)], wdc.at[mate_units, pl.ds(xx * quarter, quarter)],
+                ws.at[xx], wr.at[xx], mate_peer))
 
     def arrived(dst, sem):
         pltpu.make_async_remote_copy(
@@ -207,7 +217,7 @@
             device_id=mate_peer, device_id_type=MESH,
         ).wait_recv()
 
-    handed, ready = {}, set()
+    handed, ready, w_copies = {}, set(), []
     hop1_copies, hop2_copies = {}, {}
 
     def own_rest():
@@ -217,10 +227,19 @@
             here[:, columns] = pick(0, columns)
 
     def join(i):
-        xx = 1 - x if i else x
-        b = block(0, 1 - y, xx, c)
-        arrived(b, ar.at[i])
-        send(b, b, ams.at[i], amr.at[i], mate_peer)
+        if i == 0:
+            b = piece(1 - y, x, 0)
+            arrived(b, ar.at[0])
+            send(b, b, as_.at[3], ar.at[3], x_peer)
+            send(b, b, ams.at[0], amr.at[0], mate_peer)
+        else:
+            b = piece(1 - y, x, 1)
+            arrived(b, ar.at[1])
+            send(b, b, ams.at[1], amr.at[1], mate_peer)
+            arrived(piece(1 - y, 1 - x, 1), ar.at[2])
+            arrived(piece(1 - y, 1 - x, 0), ar.at[3])
+            b = block(0, 1 - y, 1 - x, c)
+            send(b, b, ams.at[2], amr.at[2], mate_peer)
 
     def launch(p):
         b = block(p, y, x, c)
@@ -251,8 +270,9 @@
             loads[1].wait()
         rows = rows_of(1 - y if i else y)
         if p == 0 and i == 1:
-            arrived(block(0, 1 - y, x, 1 - c), amr.at[0])
-            arrived(block(0, 1 - y, 1 - x, 1 - c), amr.at[1])
+            for b in range(2):
+                arrived(piece(1 - y, x, b), amr.at[b])
+            arrived(block(0, 1 - y, 1 - x, 1 - c), amr.at[2])
         elif p and i == 0:
             arrived(block(p, y, x, 1 - c), dr.at[p, 0])
             arrived(block(p, y, 1 - x, 1 - c), dr.at[p, 1])
@@ -321,9 +341,13 @@
         else:
             out_ref[...] = (total[...] + value).astype(bf16)
 
-    steps = dict(own_rest=own_rest, join=join, launch=launch, relay=relay, share=share, finish=finish, expand=expand,
+    steps = dict(wsend=hand_down, own_rest=own_rest, join=join, launch=launch, relay=relay, share=share, finish=finish, expand=expand,
                  shrink=shrink, second=return_second, third=return_third, mix=mix)
-    for name, *arguments in ORDER:
+    for i, (name, *arguments) in enumerate(ORDER):
+        if i == len(ORDER) - 1:
+            for copy in sent[:-3]:
+                copy.wait_send()
+            del sent[:-3]
         steps[name](*arguments)
 
     store = pltpu.make_async_copy(out_ref, out_hbm, load_sem.at[4])
@@ -378,7 +402,7 @@
             dma((5,)),
             dma((2,)), dma((2,)),
             one, one,
-            dma((2,)), dma((2,)), dma((2,)), dma((2,)),
+            dma((4,)), dma((4,)), dma((3,)), dma((3,)),
             two, two, one, one,
             dma((experts, 4)), dma((experts, 4)),
             two, two,

time: 67 us -> 62.4 us (0.931)
  Pallas kernels: 65.2 us -> 60.5 us
    pallas_call x1, Pallas kernels: 65.2 us -> 60.5 us  [fused_body(): pl.pallas_call(functools.partial(kernel, experts, cap), out_shape=jax.Sha...]
where the time goes in v2:
time: 62.4 us; the launch traced here: 62.2 us
  Pallas kernels  60.5 us (97%)
  local copies, waits for them, and re-layouts  1.67 us (3%)
    pallas_call x1, Pallas kernels, fused_body(): pl.pallas_call(functools.partial(kernel, experts, cap), out_shape=jax.Sha...  60.5 us
    unnamed x1, local copies, waits for them, and re-layouts  1.67 us

profile of v2, /device:TPU:0, one launch (start us, length us, event | category | flops | bytes accessed | tf_op | source)
XLA Modules:
  0.0 62.2 jit_solution(3522328574056186067)
XLA Ops:
  0.0 60.5 %expert_layer.1 = bf16[256,512]{1,0:T(8,128)(2,1)} custom-call(bf16[256,2048]{1,0:T(8,128)(2,1)} %tokens_ref.1, f32[1,2048]{1,0:T(1,128)} %bitcast.3, s32[2,256]{1,0:T(2,128)} %bitcast.4, f32[2,256]{1,0:T(2,128)} %bitcast.5, bf16[1,2048,896]{2,1,0:T(8,128)(2,1)} %wg_hbm.1, bf16[1,2048,896]{2,1,0:T(8,128)(2,1)} %wu_hbm.1, bf16[1,896,2048]{2,1,0:T(8,128)(2,1)} %wd_hbm.1), custom_call_target="tpu_custom_call" | custom-call | tf_op jit(solution)/shard_map/expert_layer/pallas_call | solution.py:381
  60.5 1.7 %copy.9 = bf16[256,512]{1,0:T(8,128)(2,1)} copy(bf16[256,512]{1,0:T(8,128)(2,1)} %expert_layer.1) | data formatting | bytes 524288

commit v3 on v2

--- a/solution.py
+++ b/solution.py
@@ -67,6 +67,7 @@
 )
 PARTNERS = ((2, 1, 3), (3, 0, 2))
 PICKS = (1, 0, 2, 3)
+HALF_FIRST = False
 MIXES = (1, 0, 3, 2)
 
 
@@ -87,10 +88,10 @@
     return 2 * min(tok_rows // 2, 5 * tok_rows * top_count // (8 * experts))
 
 
-def kernel(experts, cap, tokens_ref, gain_ref, ids_ref, weight_ref, wg_hbm, wu_hbm, wd_hbm,
-           out_hbm, wgu, wdc, out_ref, normed, picks, routed, away, hid, chip, hop1, turn, hop2, final, back, total,
-           load_sem, ws, wr, zs, zr, as_, ar, ams, amr, xs, xr, fs, fr, ds, dr, hs, hr,
-           h1s, h1r, h2s, h2r, bs, br):
+def kernel(experts, cap, tokens_hbm, gain_hbm, ids_hbm, weight_hbm, wg_hbm, wu_hbm, wd_hbm,
+           out_ref, tokens_ref, gain_ref, ids_ref, weight_ref, wgu, wdc, normed, spots, picks, shares, routed,
+           away, hid, chip, hop1, turn, hop2, final, back, total, span,
+           load_sem, sent_sem, wr, zr, ar, amr, xr, fr, dr, hr, h1r, h2r, br):
     ep, tp = lax.axis_index("ep"), lax.axis_index("tp")
     z, y = ep // HALVES, ep % HALVES
     x, c = tp // CORES, tp % CORES
@@ -106,17 +107,22 @@
         return pl.ds(pl.multiple_of(yy * cap, cap), cap)
 
     own_units, mate_units = pl.ds(0, units), pl.ds(units, units)
+    inputs = [
+        pltpu.make_async_copy(src, dst, load_sem.at[i])
+        for i, (src, dst) in enumerate(
+            ((tokens_hbm, tokens_ref), (ids_hbm, ids_ref), (gain_hbm, gain_ref), (weight_hbm, weight_ref)))
+    ]
+    for copy in inputs:
+        copy.start()
     loads = [
-        pltpu.make_async_copy(wg_hbm.at[0], wgu.at[:, own_units], load_sem.at[0]),
-        pltpu.make_async_copy(wu_hbm.at[0], wgu.at[:, mate_units], load_sem.at[1]),
+        pltpu.make_async_copy(wg_hbm.at[0], wgu.at[:, own_units], load_sem.at[4]),
+        pltpu.make_async_copy(wu_hbm.at[0], wgu.at[:, mate_units], load_sem.at[5]),
     ] + [
         pltpu.make_async_copy(
-            wd_hbm.at[0, :, columns_of(xx, c)], wdc.at[own_units, pl.ds(xx * quarter, quarter)], load_sem.at[2 + xx]
+            wd_hbm.at[0, :, columns_of(xx, c)], wdc.at[own_units, pl.ds(xx * quarter, quarter)], load_sem.at[6 + xx]
         )
         for xx in range(2)
     ]
-    for load in loads:
-        load.start()
 
     def device(zz, yy, xx, cc):
         return (zz * HALVES + yy, xx * CORES + cc)
@@ -133,24 +139,31 @@
     peers = [x_peer, y_peer, mate_peer] + [device(p, y, x, c) for p in plane[1:]]
     for peer in peers:
         pl.semaphore_signal(barrier, inc=1, device_id=peer, device_id_type=MESH)
-
-    ids = jnp.transpose(ids_ref[...])
-    one, two = ids[:, 0:1], ids[:, 1:2]
-    lane = lax.broadcasted_iota(jnp.int32, (tok_rows, 128), 1)
-    places = lax.broadcasted_iota(jnp.int32, (tok_rows, cap), 1)
-    expert = jnp.full((tok_rows, 128), -1, jnp.int32)
+    for load in loads:
+        load.start()
+
+    inputs[1].wait()
+    kinds = 16
+    index = lax.broadcasted_iota(jnp.int32, (kinds, tok_rows), 0)
+    expert = jnp.full((kinds, tok_rows), -1, jnp.int32)
     for k, p in enumerate(plane):
-        expert = jnp.where(lane == k, p, expert)
-    named = jnp.logical_or(one == expert, two == expert)
-    lower = (
-        lax.broadcasted_iota(jnp.int32, (tok_rows, tok_rows), 1)
-        < lax.broadcasted_iota(jnp.int32, (tok_rows, tok_rows), 0)
+        expert = jnp.where(index == k, p, expert)
+    named = jnp.logical_or(ids_ref[0:1, :] == expert, ids_ref[1:2, :] == expert)
+    earlier = (
+        lax.broadcasted_iota(jnp.int32, (tok_rows, tok_rows), 0)
+        < lax.broadcasted_iota(jnp.int32, (tok_rows, tok_rows), 1)
     )
     slot = jnp.dot(
-        lower.astype(f32).astype(bf16), named.astype(f32).astype(bf16), preferred_element_type=f32
-    )
-    slot = jnp.where(named, slot, -1.0).astype(jnp.int32)
-
+        named.astype(f32).astype(bf16), earlier.astype(f32).astype(bf16), preferred_element_type=f32
+    )
+    slot = jnp.where(named, slot, -1.0)
+    number = slot.astype(jnp.int32)
+    places = lax.broadcasted_iota(jnp.int32, (cap, tok_rows), 0)
+    for k in range(experts):
+        spots[k] = (places == number[k:k + 1, :]).astype(f32).astype(bf16)
+
+    for copy in (inputs[0], *inputs[2:]):
+        copy.wait()
     values = tokens_ref[...].astype(f32)
     mean = jnp.mean(values, axis=-1, keepdims=True)
     center = values - mean
@@ -162,23 +175,19 @@
         normed[:, columns] = (own * scale * gain_ref[:, columns]).astype(bf16)
 
     def pick(k, columns):
-        return lax.dot_general(
-            picks[k], normed[:, columns], (((0,), (0,)), ((), ())), preferred_element_type=f32
-        ).astype(bf16)
+        return jnp.dot(spots[k], normed[:, columns], preferred_element_type=f32).astype(bf16)
 
     mine = columns_of(x, c)
     norm(mine)
 
-    sent = []
-
-    def send(src, dst, send_sem, recv_sem, peer):
-        copy = pltpu.make_async_remote_copy(
-            src_ref=src, dst_ref=dst, send_sem=send_sem, recv_sem=recv_sem,
+    sizes = [0, 0]
+
+    def send(src, dst, recv_sem, peer, group=0):
+        pltpu.make_async_remote_copy(
+            src_ref=src, dst_ref=dst, send_sem=sent_sem.at[group], recv_sem=recv_sem,
             device_id=peer, device_id_type=MESH,
-        )
-        copy.start()
-        sent.append(copy)
-        return copy
+        ).start()
+        sizes[group] += src.shape[0] * src.shape[1]
 
     def block(p, yy, xx, cc):
         return routed.at[plane[p], rows_of(yy), columns_of(xx, cc)]
@@ -191,36 +200,44 @@
     here = routed.at[z, rows_of(y)]
     pl.semaphore_wait(barrier, len(peers))
     for k in PICKS:
-        picks[k] = (places == slot[:, k:k + 1]).astype(f32).astype(bf16)
         if k:
             away[k - 1] = pick(k, mine)
-            send(away.at[k - 1], routed.at[z, rows_of(y), mine], zs.at[k - 1], zr.at[z],
-                 device(plane[k], y, x, c))
+            send(away.at[k - 1], routed.at[z, rows_of(y), mine], zr.at[z], device(plane[k], y, x, c))
         else:
             here[:, mine] = pick(0, mine)
             for i in range(2):
-                send(piece(y, x, i), piece(y, x, i), as_.at[i], ar.at[i], y_peer)
+                send(piece(y, x, i), piece(y, x, i), ar.at[i], y_peer)
     norm(columns_of(1 - x, c))
     here[:, columns_of(1 - x, c)] = pick(0, columns_of(1 - x, c))
     b = piece(y, 1 - x, 1)
-    send(b, b, as_.at[2], ar.at[2], y_peer)
+    send(b, b, ar.at[2], y_peer)
 
     def hand_down():
         for xx in range(2):
-            w_copies.append(send(
-                wd_hbm.at[0, :, columns_of(xx, 1 - c)], wdc.at[mate_units, pl.ds(xx * quarter, quarter)],
-                ws.at[xx], wr.at[xx], mate_peer))
+            send(wd_hbm.at[0, :, columns_of(xx, 1 - c)], wdc.at[mate_units, pl.ds(xx * quarter, quarter)],
+                 wr.at[0], mate_peer, 1)
 
     def arrived(dst, sem):
         pltpu.make_async_remote_copy(
-            src_ref=dst, dst_ref=dst, send_sem=zs.at[0], recv_sem=sem,
+            src_ref=dst, dst_ref=dst, send_sem=sent_sem.at[0], recv_sem=sem,
             device_id=mate_peer, device_id_type=MESH,
         ).wait_recv()
 
-    handed, ready, w_copies = {}, set(), []
-    hop1_copies, hop2_copies = {}, {}
+    ready = set()
 
     def own_rest():
+        ids, route = jnp.transpose(ids_ref[...]), jnp.transpose(weight_ref[...])
+        lane = lax.broadcasted_iota(jnp.int32, shares.shape, 1)
+        expert = jnp.full(shares.shape, -1, jnp.int32)
+        for k, p in enumerate(plane):
+            expert = jnp.where(lane == k, p, expert)
+        shares[...] = (
+            jnp.where(ids[:, 0:1] == expert, route[:, 0:1], 0.0) + jnp.where(ids[:, 1:2] == expert, route[:, 1:2], 0.0)
+        )
+        number = jnp.transpose(slot).astype(jnp.int32)
+        places = lax.broadcasted_iota(jnp.int32, (tok_rows, cap), 1)
+        for k in range(experts):
+            picks[k] = (places == number[:, k:k + 1]).astype(f32).astype(bf16)
         for xx in (x, 1 - x):
             columns = columns_of(xx, 1 - c)
             norm(columns)
@@ -230,39 +247,39 @@
         if i == 0:
             b = piece(1 - y, x, 0)
             arrived(b, ar.at[0])
-            send(b, b, as_.at[3], ar.at[3], x_peer)
-            send(b, b, ams.at[0], amr.at[0], mate_peer)
+            send(b, b, ar.at[3], x_peer)
+            send(b, b, amr.at[0], mate_peer)
         else:
             b = piece(1 - y, x, 1)
             arrived(b, ar.at[1])
-            send(b, b, ams.at[1], amr.at[1], mate_peer)
+            send(b, b, amr.at[0], mate_peer)
             arrived(piece(1 - y, 1 - x, 1), ar.at[2])
             arrived(piece(1 - y, 1 - x, 0), ar.at[3])
             b = block(0, 1 - y, 1 - x, c)
-            send(b, b, ams.at[2], amr.at[2], mate_peer)
+            send(b, b, amr.at[0], mate_peer)
 
     def launch(p):
         b = block(p, y, x, c)
         arrived(b, zr.at[plane[p]])
-        send(b, b, xs.at[p, 0], xr.at[p, 0], x_peer)
-        send(b, b, xs.at[p, 1], xr.at[p, 1], y_peer)
-        send(b, b, ds.at[p, 0], dr.at[p, 0], mate_peer)
+        send(b, b, xr.at[p - 1, 0], x_peer)
+        send(b, b, xr.at[p - 1, 1], y_peer)
+        send(b, b, dr.at[p - 1, 0], mate_peer)
 
     def relay(p):
         b = block(p, c * y + (1 - c) * (1 - y), c * (1 - x) + (1 - c) * x, c)
-        arrived(b, xr.at[p, 1 - c])
-        send(b, b, fs.at[p], fr.at[p], first)
-        send(b, b, ds.at[p, 2 - c], dr.at[p, 2 - c], mate_peer)
+        arrived(b, xr.at[p - 1, 1 - c])
+        send(b, b, fr.at[p - 1], first)
+        send(b, b, dr.at[p - 1, 1 - c], mate_peer)
 
     def share(p):
         b = block(p, (1 - c) * y + c * (1 - y), (1 - c) * (1 - x) + c * x, c)
-        arrived(b, xr.at[p, c])
-        send(b, b, ds.at[p, 1 + c], dr.at[p, 1 + c], mate_peer)
+        arrived(b, xr.at[p - 1, c])
+        send(b, b, dr.at[p - 1, c], mate_peer)
 
     def finish(p):
         b = block(p, 1 - y, 1 - x, c)
-        arrived(b, fr.at[p])
-        send(b, b, ds.at[p, 3], dr.at[p, 3], mate_peer)
+        arrived(b, fr.at[p - 1])
+        send(b, b, dr.at[p - 1, 1], mate_peer)
 
     def expand(p, i):
         if p == 0 and i == 0:
@@ -270,32 +287,22 @@
             loads[1].wait()
         rows = rows_of(1 - y if i else y)
         if p == 0 and i == 1:
-            for b in range(2):
-                arrived(piece(1 - y, x, b), amr.at[b])
-            arrived(block(0, 1 - y, 1 - x, 1 - c), amr.at[2])
-        elif p and i == 0:
-            arrived(block(p, y, x, 1 - c), dr.at[p, 0])
-            arrived(block(p, y, 1 - x, 1 - c), dr.at[p, 1])
+            arrived(routed.at[z, rows_of(1 - y), pl.ds(0, 2 * quarter)], amr.at[0])
         elif p:
-            arrived(block(p, 1 - y, x, 1 - c), dr.at[p, 2])
-            arrived(block(p, 1 - y, 1 - x, 1 - c), dr.at[p, 3])
+            arrived(routed.at[plane[p], rows, pl.ds(0, 2 * quarter)], dr.at[p - 1, i])
         both = jnp.dot(routed[plane[p], rows], wgu[...], preferred_element_type=f32)
         gate, up = both[:, :units], both[:, units:]
         hid[p, rows, own_units] = (gate / (1.0 + jnp.exp(-gate)) * up).astype(bf16)
-        handed[p, i] = send(
-            hid.at[p, rows, own_units], hid.at[p, rows, mate_units], hs.at[p, i], hr.at[p, i], mate_peer
-        )
+        send(hid.at[p, rows, own_units], hid.at[p, rows, mate_units], hr.at[p], mate_peer, 1)
 
     def shrink(p, js):
         if not ready:
             for copy in loads[2:]:
                 copy.wait()
-            for copy in w_copies:
-                copy.wait_recv()
+            arrived(wdc.at[mate_units], wr.at[0])
         if p not in ready:
             ready.add(p)
-            for i in range(2):
-                handed[p, i].wait_recv()
+            arrived(hid.at[p, :, mate_units], hr.at[p])
         for j in js:
             low, high = j % 2, j // 2
             x_low, x_high = (1 - x if low else x), (1 - x if high else x)
@@ -307,33 +314,29 @@
                 preferred_element_type=f32,
             ).astype(bf16)
             if j >= 2:
-                hop1_copies[p, j - 2] = send(
-                    chip.at[p, j], hop1.at[p, j - 2], h1s.at[p, j - 2], h1r.at[p, j - 2], first
-                )
+                send(chip.at[p, j], hop1.at[p, j - 2], h1r.at[p, j - 2], first, 1)
 
     def return_second(p):
-        hop1_copies[p, 1].wait_recv()
+        arrived(hop1.at[p, 1], h1r.at[p, 1])
         turn[p] = (chip[p, 1].astype(f32) + hop1[p, 1].astype(f32)).astype(bf16)
-        hop2_copies[p] = send(turn.at[p], hop2.at[p], h2s.at[p], h2r.at[p], second)
+        send(turn.at[p], hop2.at[p], h2r.at[p], second, 1)
 
     def return_third(p):
-        hop1_copies[p, 0].wait_recv()
+        arrived(hop1.at[p, 0], h1r.at[p, 0])
         part = chip[p, 0].astype(f32) + hop1[p, 0].astype(f32)
-        hop2_copies[p].wait_recv()
+        arrived(hop2.at[p], h2r.at[p])
         part = (part + hop2[p].astype(f32)).astype(bf16)
         if p == 0:
             back[z] = part
         else:
             final[p - 1] = part
-            send(final.at[p - 1], back.at[z], bs.at[p - 1], br.at[z], device(plane[p], y, x, c))
+            send(final.at[p - 1], back.at[z], br.at[z], device(plane[p], y, x, c), 1)
 
     def mix(p):
         e = plane[p]
         if p:
             arrived(back.at[e], br.at[e])
-        route = jnp.transpose(weight_ref[...])
-        share = jnp.where(one == e, route[:, 0:1], 0.0) + jnp.where(two == e, route[:, 1:2], 0.0)
-        value = share * jnp.dot(picks[p], back[e], preferred_element_type=f32)
+        value = shares[:, p:p + 1] * jnp.dot(picks[p], back[e], preferred_element_type=f32)
         if p == MIXES[0]:
             total[...] = value
         elif p != MIXES[-1]:
@@ -345,16 +348,10 @@
                  shrink=shrink, second=return_second, third=return_third, mix=mix)
     for i, (name, *arguments) in enumerate(ORDER):
         if i == len(ORDER) - 1:
-            for copy in sent[:-3]:
-                copy.wait_send()
-            del sent[:-3]
+            for g in range(2):
+                whole = span.at[pl.ds(0, sizes[g] // quarter)]
+                pltpu.make_async_copy(whole, whole, sent_sem.at[g]).wait()
         steps[name](*arguments)
-
-    store = pltpu.make_async_copy(out_ref, out_hbm, load_sem.at[4])
-    store.start()
-    for copy in sent:
-        copy.wait_send()
-    store.wait()
 
 
 def nearest(z, k, experts):
@@ -377,21 +374,26 @@
     dma = pltpu.SemaphoreType.DMA
     vmem = pl.BlockSpec(memory_space=pltpu.VMEM)
     hbm = pl.BlockSpec(memory_space=pl.ANY)
-    one, two = dma((experts,)), dma((experts, 2))
+    rows = HALVES * cap
     return pl.pallas_call(
         functools.partial(kernel, experts, cap),
-        out_shape=jax.ShapeDtypeStruct((tok_rows, quarter), bf16),
-        in_specs=[vmem, vmem, vmem, vmem, hbm, hbm, hbm],
-        out_specs=hbm,
+        out_shape=pltpu.VMEM((tok_rows, quarter), bf16),
+        in_specs=[hbm] * 7,
+        out_specs=vmem,
         scratch_shapes=[
+            pltpu.VMEM(tokens.shape, bf16),
+            pltpu.VMEM((1, width), jnp.float32),
+            pltpu.VMEM(expert_ids.shape[::-1], jnp.int32),
+            pltpu.VMEM(route_weight.shape[::-1], jnp.float32),
             pltpu.VMEM((width, 2 * units), bf16),
             pltpu.VMEM((CORES * units, 2 * quarter), bf16),
-            pltpu.VMEM((tok_rows, quarter), bf16),
             pltpu.VMEM((tok_rows, width), bf16),
+            pltpu.VMEM((experts, cap, tok_rows), bf16),
             pltpu.VMEM((experts, tok_rows, cap), bf16),
-            pltpu.VMEM((experts, HALVES * cap, width), bf16),
+            pltpu.VMEM((tok_rows, 128), jnp.float32),
+            pltpu.VMEM((experts, rows, width), bf16),
             pltpu.VMEM((experts - 1, cap, quarter), bf16),
-            pltpu.VMEM((experts, HALVES * cap, CORES * units), bf16),
+            pltpu.VMEM((experts, rows, CORES * units), bf16),
             pltpu.VMEM((experts, 4, cap, quarter), bf16),
             pltpu.VMEM((experts, 2, cap, quarter), bf16),
             pltpu.VMEM((experts, cap, quarter), bf16),
@@ -399,14 +401,11 @@
             pltpu.VMEM((experts - 1, cap, quarter), bf16),
             pltpu.VMEM((experts, cap, quarter), bf16),
             pltpu.VMEM((tok_rows, quarter), jnp.float32),
-            dma((5,)),
-            dma((2,)), dma((2,)),
-            one, one,
-            dma((4,)), dma((4,)), dma((3,)), dma((3,)),
-            two, two, one, one,
-            dma((experts, 4)), dma((experts, 4)),
-            two, two,
-            two, two, one, one, one, one,
+            pltpu.VMEM((8 * experts * rows, quarter), bf16),
+            dma((8,)), dma((2,)),
+            dma((1,)), dma((experts,)), dma((4,)), dma((1,)),
+            dma((experts - 1, 2)), dma((experts - 1,)), dma((experts - 1, 2)), dma((experts,)),
+            dma((experts, 2)), dma((experts,)), dma((experts,)),
         ],
         compiler_params=pltpu.CompilerParams(
             collective_id=0, has_side_effects=True, vmem_limit_bytes=60 * 1024 * 1024

time: 62.4 us -> 58.7 us (0.941)
  Pallas kernels: 60.5 us -> 57.9 us
  local copies, waits for them, and re-layouts: 1.67 us -> 0.71 us
    pallas_call x1, Pallas kernels: 60.5 us -> 57.9 us  [fused_body(): pl.pallas_call(functools.partial(kernel, experts, cap), out_shape=pltpu.V...]
    unnamed x1, local copies, waits for them, and re-layouts: 1.67 us -> 0.71 us
where the time goes in v3:
time: 58.7 us; the launch traced here: 58.6 us
  Pallas kernels  57.9 us (99%)
  local copies, waits for them, and re-layouts  0.71 us (1%)
    pallas_call x1, Pallas kernels, fused_body(): pl.pallas_call(functools.partial(kernel, experts, cap), out_shape=pltpu.V...  57.9 us

profile of v3, /device:TPU:0, one launch (start us, length us, event | category | flops | bytes accessed | tf_op | source)
XLA Modules:
  0.0 58.6 jit_solution(7021871987372346304)
XLA Ops:
  0.0 57.9 %expert_layer.1 = bf16[256,512]{1,0:T(8,128)(2,1)S(1)} custom-call(bf16[256,2048]{1,0:T(8,128)(2,1)} %tokens_hbm.1, f32[1,2048]{1,0:T(1,128)} %bitcast.3, s32[2,256]{1,0:T(2,128)} %bitcast.4, f32[2,256]{1,0:T(2,128)} %bitcast.5, bf16[1,2048,896]{2,1,0:T(8,128)(2,1)} %wg_hbm.1, bf16[1,2048,896]{2,1,0:T(8,128)(2,1)} %wu_hbm.1, bf16[1,896,2048]{2,1,0:T(8,128)(2,1)} %wd_hbm.1), custom_call_target="tpu_custom_call" | custom-call | tf_op jit(solution)/shard_map/expert_layer/pallas_call | solution.py:378
  57.9 0.7 %copy.9 = bf16[256,512]{1,0:T(8,128)(2,1)} copy(bf16[256,512]{1,0:T(8,128)(2,1)S(1)} %expert_layer.1) | data formatting | bytes 524288

commit v4 on v3

--- a/solution.py
+++ b/solution.py
@@ -12,63 +12,65 @@
 EPSILON = 1e-05
 MESH = pl.DeviceIdType.MESH
 ORDER = (
+    ('own_rest',),
     ('join', 0),
-    ('own_rest',),
+    ('wsend',),
+    ('dispatch', 1),
     ('launch', 1),
+    ('expand', 0, 0),
     ('join', 1),
-    ('wsend',),
-    ('expand', 0, 0),
+    ('dispatch', 3),
     ('launch', 2),
     ('expand', 0, 1),
+    ('share', 1),
     ('relay', 1),
-    ('share', 1),
     ('expand', 1, 0),
+    ('relay', 2),
+    ('finish', 1),
+    ('shrink', 0, (1,)),
     ('launch', 3),
-    ('finish', 1),
+    ('expand', 1, 1),
     ('shrink', 0, (0,)),
-    ('relay', 2),
     ('share', 2),
-    ('expand', 1, 1),
+    ('shrink', 1, (3,)),
+    ('finish', 2),
+    ('expand', 2, 0),
+    ('relay', 3),
+    ('expand', 2, 1),
+    ('shrink', 1, (2,)),
     ('share', 3),
-    ('relay', 3),
-    ('shrink', 1, (3,)),
-    ('shrink', 1, (2,)),
+    ('shrink', 2, (3,)),
+    ('shrink', 1, (1,)),
+    ('shrink', 1, (0,)),
+    ('shrink', 2, (1,)),
+    ('second', 1),
+    ('finish', 3),
     ('expand', 3, 0),
-    ('shrink', 1, (1,)),
-    ('finish', 2),
-    ('finish', 3),
-    ('expand', 2, 0),
-    ('second', 1),
+    ('shrink', 2, (2,)),
     ('expand', 3, 1),
-    ('shrink', 0, (3,)),
-    ('shrink', 1, (0,)),
+    ('second', 2),
+    ('third', 1),
     ('shrink', 3, (3,)),
-    ('third', 1),
     ('shrink', 3, (2,)),
+    ('shrink', 2, (0,)),
+    ('third', 2),
     ('shrink', 3, (1,)),
-    ('shrink', 0, (1,)),
-    ('expand', 2, 1),
     ('second', 3),
     ('shrink', 3, (0,)),
-    ('shrink', 2, (1,)),
-    ('shrink', 2, (3,)),
-    ('shrink', 2, (2,)),
+    ('mix', 2),
+    ('shrink', 0, (3,)),
+    ('shrink', 0, (2,)),
     ('third', 3),
-    ('second', 2),
     ('second', 0),
-    ('shrink', 2, (0,)),
     ('mix', 1),
-    ('shrink', 0, (2,)),
-    ('third', 2),
     ('third', 0),
     ('mix', 0),
     ('mix', 3),
-    ('mix', 2),
 )
-PARTNERS = ((2, 1, 3), (3, 0, 2))
-PICKS = (1, 0, 2, 3)
+PARTNERS = ((2, 1, 3), (0, 3, 2))
+PICKS = (2, 0)
 HALF_FIRST = False
-MIXES = (1, 0, 3, 2)
+MIXES = (2, 1, 0, 3)
 
 
 def layer_normed(tokens, norm_gain):
@@ -197,12 +199,15 @@
     def piece(yy, xx, i):
         return routed.at[z, pl.ds(pl.multiple_of(yy * cap + i * half, half), half), columns_of(xx, c)]
 
+    def dispatch(k):
+        away[k - 1] = pick(k, mine)
+        send(away.at[k - 1], routed.at[z, rows_of(y), mine], zr.at[z], device(plane[k], y, x, c))
+
     here = routed.at[z, rows_of(y)]
     pl.semaphore_wait(barrier, len(peers))
     for k in PICKS:
         if k:
-            away[k - 1] = pick(k, mine)
-            send(away.at[k - 1], routed.at[z, rows_of(y), mine], zr.at[z], device(plane[k], y, x, c))
+            dispatch(k)
         else:
             here[:, mine] = pick(0, mine)
             for i in range(2):
@@ -344,7 +349,7 @@
         else:
             out_ref[...] = (total[...] + value).astype(bf16)
 
-    steps = dict(wsend=hand_down, own_rest=own_rest, join=join, launch=launch, relay=relay, share=share, finish=finish, expand=expand,
+    steps = dict(dispatch=dispatch, wsend=hand_down, own_rest=own_rest, join=join, launch=launch, relay=relay, share=share, finish=finish, expand=expand,
                  shrink=shrink, second=return_second, third=return_third, mix=mix)
     for i, (name, *arguments) in enumerate(ORDER):
         if i == len(ORDER) - 1:

time: 58.7 us -> 58.2 us (level)
  Pallas kernels: 57.9 us -> 57.3 us
where the time goes in v4:
time: 58.2 us; the launch traced here: 58.1 us
  Pallas kernels  57.3 us (98%)
  local copies, waits for them, and re-layouts  0.71 us (1%)
    pallas_call x1, Pallas kernels, fused_body(): pl.pallas_call(functools.partial(kernel, experts, cap), out_shape=pltpu.V...  57.3 us

profile of v4, /device:TPU:0, one launch (start us, length us, event | category | flops | bytes accessed | tf_op | source)
XLA Modules:
  0.0 58.1 jit_solution(1050101621623935547)
XLA Ops:
  0.0 57.3 %expert_layer.1 = bf16[256,512]{1,0:T(8,128)(2,1)S(1)} custom-call(bf16[256,2048]{1,0:T(8,128)(2,1)} %tokens_hbm.1, f32[1,2048]{1,0:T(1,128)} %bitcast.3, s32[2,256]{1,0:T(2,128)} %bitcast.4, f32[2,256]{1,0:T(2,128)} %bitcast.5, bf16[1,2048,896]{2,1,0:T(8,128)(2,1)} %wg_hbm.1, bf16[1,2048,896]{2,1,0:T(8,128)(2,1)} %wu_hbm.1, bf16[1,896,2048]{2,1,0:T(8,128)(2,1)} %wd_hbm.1), custom_call_target="tpu_custom_call" | custom-call | tf_op jit(solution)/shard_map/expert_layer/pallas_call | solution.py:383
  57.4 0.7 %copy.9 = bf16[256,512]{1,0:T(8,128)(2,1)} copy(bf16[256,512]{1,0:T(8,128)(2,1)S(1)} %expert_layer.1) | data formatting | bytes 524288
